TPU v7x, 32 devices: a whole 2x2x4 slice. The times are simulated.
32 devices in a mesh: sp: 8 (over z, x), dp: 4 (over y, core).
Axes of the slice: x: 2, y: 2, z: 4, core: 2. Of those that a mesh axis runs over, the one named last changes fastest.
Arguments:
- residual_in: bfloat16 [4, 1024, 2048], P('dp', 'sp'), may hold values from -6 to 6
- ssm_input: bfloat16 [4, 1024, 2048], P('dp', 'sp'), may hold values from -6 to 6
- state_b: bfloat16 [4, 1024, 2048], P('dp', 'sp'), may hold values from -6 to 6
- state_c: bfloat16 [4, 1024, 2048], P('dp', 'sp'), may hold values from -6 to 6
- step_raw: bfloat16 [4, 1024, 64], P('dp', 'sp'), may hold values from -4 to 3
- gate_input: bfloat16 [4, 1024, 2048], P('dp', 'sp'), may hold values from -6 to 6
- conv_x: float32 [7, 2048], P(None, 'sp'), may hold values from -2 to 2
- conv_b: float32 [7, 2048], P(None, 'sp'), may hold values from -2 to 2
- conv_c: float32 [7, 2048], P(None, 'sp'), may hold values from -2 to 2
- decay_rate: float32 [2, 32], P(None, 'sp'), may hold values from 0 to 1, as said below
- mix_gain: float32 [2048], replicated, may hold values from 0.1 to 1.9
- out_weight: bfloat16 [2048, 2048], P('dp'), may hold values from -0.125 to 0.125
- ffn_gain: float32 [2048], replicated, may hold values from 0.1 to 1.9
- routing: int32 [4, 1024, 4], P('dp', 'sp'), may hold values from 0 to 31, all different within a row; in each aligned block of 128 rows (0 to 127, 128 to 255, ..., all dimensions but the last counted through in order) at most 32 rows name the same one
- route_weight: float32 [4, 1024, 4], P('dp', 'sp'), may hold values from 0.1 to 0.6
- gate_w: bfloat16 [32, 2048, 1024], P(('sp', 'dp')), may hold values from -60 to 60
- up_w: bfloat16 [32, 2048, 1024], P(('sp', 'dp')), may hold values from -60 to 60
- down_w: bfloat16 [32, 1024, 2048], P(('sp', 'dp')), may hold values from -0.1875 to 0.1875
Outputs:
- block_out: bfloat16 [4, 1024, 2048], P('dp', 'sp')
Inputs may be any that keep to these rules, and one draw needn't show every extreme that they name: `routing`: each row names 4 different experts; within the rows of one device no expert is named by more than 32 rows, a bound that some block reaches. `decay_rate`: Positive.
All inputs are finite; a program needn't handle non-finite values.
Results may differ from a plain program's by a relative error of at most 0.0082.
Values may be sent and summed in bfloat16 or wider, within the bound.
No kernel may reach another device: no remote copies, remote signals or barrier semaphores. Data moves between devices by JAX's collectives and lax.ppermute only.
A program may use at most 128 MiB of HBM per device.

v0:
```python
import jax
import jax.numpy as jnp
from jax import lax
from jax.sharding import PartitionSpec as P

HEAD_DIM = 64
STATE = 128
BLOCK = 128
NORM_GROUPS = 4
highest = lax.Precision.HIGHEST
epsilon = 1e-05
clamp_limit = 7.0
sigmoid_slope = 1.702


def centred_conv(values, taps):
    half_width = taps.shape[0] // 2
    padded = jnp.pad(values, ((half_width, half_width), (0, 0)))
    total = jnp.zeros_like(values)
    for offset in range(taps.shape[0]):
        total = total + padded[offset : offset + values.shape[0]] * taps[offset]
    return total


def ssd_direction(signal, step_size, rates, write_map, read_map):
    length = signal.shape[0]
    head_count = signal.shape[1]
    head_width = signal.shape[2]
    group_count = write_map.shape[1]
    state_width = write_map.shape[2]
    per_group = head_count // group_count
    blocks = length // BLOCK
    scaled = (signal * step_size[..., None]).reshape(
        blocks, BLOCK, group_count, per_group, head_width
    )
    cumulative = jnp.cumsum(
        (-step_size * rates).reshape(blocks, BLOCK, group_count, per_group), axis=1
    )
    write_block = write_map.reshape(blocks, BLOCK, group_count, state_width)
    read_block = read_map.reshape(blocks, BLOCK, group_count, state_width)
    spread = cumulative[:, :, None] - cumulative[:, None]
    lower_mask = (lax.iota(jnp.int32, BLOCK)[:, None] >= lax.iota(jnp.int32, BLOCK)[None, :])[
        None, :, :, None, None
    ]
    weight_in = jnp.exp(jnp.where(lower_mask, spread, -jnp.inf))
    intersect = jnp.einsum("clgn,csgn->clsg", read_block, write_block, precision=highest)
    inside = jnp.einsum(
        "clsgk,csgkp->clgkp", intersect[..., None] * weight_in, scaled, precision=highest
    )
    to_end = jnp.exp(cumulative[:, -1:] - cumulative)
    states = jnp.einsum(
        "csgn,csgkp->cgkpn", write_block, scaled * to_end[..., None], precision=highest
    )
    carry_decay = jnp.exp(cumulative[:, -1])

    def advance(running, block_pair):
        block_state, factor = block_pair
        return (factor[..., None, None] * running + block_state, running)

    initial = jnp.zeros((group_count, per_group, head_width, state_width), jnp.float32)
    _, entering = lax.scan(advance, initial, (states, carry_decay))
    carried = (
        jnp.einsum("clgn,cgkpn->clgkp", read_block, entering, precision=highest)
        * jnp.exp(cumulative)[..., None]
    )
    return (inside + carried).reshape(length, head_count, head_width)


def both_ways(signal, steps_fwd, steps_bwd, rates, write_map, read_map):
    forward = ssd_direction(signal, steps_fwd, rates[0], write_map, read_map)
    backward = ssd_direction(
        jnp.flip(signal, 0),
        jnp.flip(steps_bwd, 0),
        rates[1],
        jnp.flip(write_map, 0),
        jnp.flip(read_map, 0),
    )
    return forward + jnp.flip(backward, 0)


def scale_rows(values, gains):
    return values * lax.rsqrt(jnp.mean(values * values, axis=-1, keepdims=True) + epsilon) * gains


def group_scale(values, gains):
    shaped = values.reshape(values.shape[:-1] + (NORM_GROUPS, values.shape[-1] // NORM_GROUPS))
    shaped = shaped * lax.rsqrt(jnp.mean(shaped * shaped, axis=-1, keepdims=True) + epsilon)
    return shaped.reshape(values.shape) * gains


def expert_apply(rows, gate_mat, up_mat, down_mat):
    gate_value = jnp.minimum(
        jnp.dot(rows, gate_mat, preferred_element_type=jnp.float32), clamp_limit
    )
    up_value = jnp.clip(
        jnp.dot(rows, up_mat, preferred_element_type=jnp.float32), -clamp_limit, clamp_limit
    )
    active = ((up_value + 1.0) * gate_value * jax.nn.sigmoid(sigmoid_slope * gate_value)).astype(
        jnp.bfloat16
    )
    return jnp.dot(active, down_mat, preferred_element_type=jnp.float32).astype(jnp.bfloat16)


def per_device(
    residual_in,
    ssm_input,
    state_b,
    state_c,
    step_raw,
    gate_input,
    conv_x,
    conv_b,
    conv_c,
    decay_rate,
    mix_gain,
    out_weight,
    ffn_gain,
    routing,
    route_weight,
    gate_w,
    up_w,
    down_w,
):
    signal_loc, write_loc, read_loc, step_loc = (
        lax.all_to_all(ssm_input, "sp", split_axis=2, concat_axis=1, tiled=True),
        lax.all_to_all(state_b, "sp", split_axis=2, concat_axis=1, tiled=True),
        lax.all_to_all(state_c, "sp", split_axis=2, concat_axis=1, tiled=True),
        lax.all_to_all(step_raw, "sp", split_axis=2, concat_axis=1, tiled=True),
    )
    length = signal_loc.shape[1]
    head_local = decay_rate.shape[1]
    signal = jax.nn.silu(centred_conv(signal_loc[0].astype(jnp.float32), conv_x)).reshape(
        length, head_local, HEAD_DIM
    )
    write_map = jax.nn.silu(centred_conv(write_loc[0].astype(jnp.float32), conv_b)).reshape(
        length, -1, STATE
    )
    read_map = jax.nn.silu(centred_conv(read_loc[0].astype(jnp.float32), conv_c)).reshape(
        length, -1, STATE
    )
    step_pair = jax.nn.softplus(step_loc[0].astype(jnp.float32).reshape(length, head_local, 2))
    mixed_heads = both_ways(
        signal, step_pair[..., 0], step_pair[..., 1], decay_rate, write_map, read_map
    )
    mixed_heads = mixed_heads.reshape(1, length, head_local * HEAD_DIM).astype(jnp.bfloat16)
    mixed_tokens = lax.all_to_all(mixed_heads, "sp", split_axis=1, concat_axis=2, tiled=True)
    token_count = residual_in.shape[1]
    model_width = residual_in.shape[2]
    gated = mixed_tokens[0].astype(jnp.float32) * jax.nn.silu(gate_input[0].astype(jnp.float32))
    mixed = group_scale(gated, mix_gain).astype(jnp.bfloat16)
    projected = jnp.dot(
        mixed,
        lax.all_gather(out_weight, "dp", axis=0, tiled=True),
        preferred_element_type=jnp.float32,
    )
    stream = residual_in[0].astype(jnp.float32) + projected
    ffn_input = scale_rows(stream, ffn_gain).astype(jnp.bfloat16)
    sp_count = lax.axis_size("sp")
    dp_count = lax.axis_size("dp")
    experts_all = sp_count * dp_count
    top_count = routing.shape[2]
    assigned = token_count * top_count
    capacity = 2 * assigned // experts_all
    flat_expert = routing.reshape(assigned)
    one_hot = (flat_expert[:, None] == lax.iota(jnp.int32, experts_all)[None, :]).astype(
        jnp.bfloat16
    )
    earlier = (
        lax.iota(jnp.int32, assigned)[:, None] > lax.iota(jnp.int32, assigned)[None, :]
    ).astype(jnp.bfloat16)
    before = jnp.dot(earlier, one_hot, preferred_element_type=jnp.float32)
    slot_index = jnp.sum(before * one_hot.astype(jnp.float32), axis=1).astype(jnp.int32)
    target = flat_expert * capacity + slot_index
    source_token = (
        jnp.zeros((experts_all * capacity,), jnp.int32)
        .at[target]
        .set(lax.iota(jnp.int32, assigned) // top_count)
    )
    filled = jnp.zeros((experts_all * capacity,), jnp.bool_).at[target].set(True)
    outgoing = jnp.where(filled[:, None], ffn_input[source_token], jnp.zeros((), jnp.bfloat16))
    arrived = lax.all_to_all(
        outgoing.reshape(experts_all, 1, capacity, model_width),
        ("sp", "dp"),
        split_axis=0,
        concat_axis=1,
        tiled=True,
    )
    served = expert_apply(arrived.reshape(-1, model_width), gate_w[0], up_w[0], down_w[0]).reshape(
        arrived.shape
    )
    returned = lax.all_to_all(served, ("sp", "dp"), split_axis=1, concat_axis=0, tiled=True)
    answers = returned.reshape(experts_all * capacity, model_width)[target].reshape(
        token_count, top_count, model_width
    )
    routed = jnp.sum(answers.astype(jnp.float32) * route_weight[0][:, :, None], axis=1)
    return (stream + routed).astype(jnp.bfloat16)[None]


def solution(mesh):
    return jax.shard_map(
        per_device,
        mesh=mesh,
        in_specs=(
            P("dp", "sp", None),
            P("dp", "sp", None),
            P("dp", "sp", None),
            P("dp", "sp", None),
            P("dp", "sp", None),
            P("dp", "sp", None),
            P(None, "sp"),
            P(None, "sp"),
            P(None, "sp"),
            P(None, "sp"),
            P(),
            P("dp", None),
            P(),
            P("dp", "sp", None),
            P("dp", "sp", None),
            P(("sp", "dp"), None, None),
            P(("sp", "dp"), None, None),
            P(("sp", "dp"), None, None),
        ),
        out_specs=P("dp", "sp", None),
        check_vma=False,
    )
```

profile of v0, /device:TPU:0, one launch (start us, length us, event | category | flops | bytes accessed | tf_op | source)
XLA Modules:
  0.0 593.2 jit_solution(14544832548649737198)
XLA Ops:
  9.2 7.3 %all-to-all-start.1 = ((bf16[8,2,512]{2,1,0:T(2,128)(2,1)}), bf16[8,2,512]{2,1,0:T(2,128)(2,1)S(1)}, u32[]{:S(2)}, u32[]{:S(2)}) async-start(bf16[8,2,512]{2,1,0:T(2,128)(2,1)} %reshape.329), calls=%async_computation.1 | async-start | bytes 32768 | tf_op jit(solution)/shard_map/all_to_all | solution.py:128
  25.2 11.5 %reduce.8 = bf16[2048,128]{1,0:T(8,128)(2,1)S(1)} reduce(bf16[2048,1,128]{2,1,0:T(2,128)(2,1)S(1)} %bitcast.256, bf16[]{:T(256)} %broadcast.189), dimensions={1}, to_apply=%bitcast.193.reduce_sub_computation | reduce | bytes 1048578
  38.4 11.5 %reduce.7 = bf16[2048,128]{1,0:T(8,128)(2,1)S(1)} reduce(bf16[2048,1,128]{2,1,0:T(2,128)(2,1)S(1)} %bitcast.257, bf16[]{:T(256)} %broadcast.189), dimensions={1}, to_apply=%bitcast.191.reduce_sub_computation | reduce | bytes 1048578
  51.6 11.8 %reduce.9 = bf16[2048,128]{1,0:T(8,128)(2,1)S(1)} reduce(bf16[2048,1,128]{2,1,0:T(2,128)(2,1)S(1)} %bitcast.258, bf16[]{:T(256)} %broadcast.189), dimensions={1}, to_apply=%bitcast.195.reduce_sub_computation | reduce | bytes 1048578
  64.4 6.0 %all-to-all-start = ((bf16[8,2,16384]{2,1,0:T(2,128)(2,1)}), bf16[8,2,16384]{2,1,0:T(2,128)(2,1)}, u32[]{:S(2)}, u32[]{:S(2)}) async-start(bf16[8,2,16384]{2,1,0:T(2,128)(2,1)} %reshape.333), calls=%async_computation | async-start | bytes 1048576 | tf_op jit(solution)/shard_map/all_to_all | solution.py:125
  71.8 47.4 %fusion.95 = f32[8,128,2,2]{3,0,1,2:T(8,128)S(1)} fusion(f32[8,128,2,2]{3,0,1,2:T(8,128)S(1)} %copy.202), kind=kOutput, calls=%fused_computation.155 | output fusion | flops 520192 | bytes 32768 | tf_op jit(solution)/shard_map/jit(cumsum)/reduce_window_sum | solution.py:36
  120.0 47.4 %fusion.94 = f32[8,128,2,2]{3,0,1,2:T(8,128)S(1)} fusion(f32[8,128,2,2]{3,0,1,2:T(8,128)S(1)} %copy.183), kind=kOutput, calls=%fused_computation.154 | output fusion | flops 520192 | bytes 32768 | tf_op jit(solution)/shard_map/jit(cumsum)/reduce_window_sum | solution.py:36
  170.5 6.0 %all-to-all-start.2 = ((bf16[8,2,16384]{2,1,0:T(2,128)(2,1)}), bf16[8,2,16384]{2,1,0:T(2,128)(2,1)}, u32[]{:S(2)}, u32[]{:S(2)}) async-start(bf16[8,2,16384]{2,1,0:T(2,128)(2,1)} %reshape.331), calls=%async_computation.2 | async-start | bytes 1048576 | tf_op jit(solution)/shard_map/all_to_all | solution.py:126
  190.0 6.2 %all-to-all-start.3 = ((bf16[8,2,16384]{2,1,0:T(2,128)(2,1)}), bf16[8,2,16384]{2,1,0:T(2,128)(2,1)}, u32[]{:S(2)}, u32[]{:S(2)}) async-start(bf16[8,2,16384]{2,1,0:T(2,128)(2,1)} %reshape.335), calls=%async_computation.3 | async-start | bytes 1048576 | tf_op jit(solution)/shard_map/all_to_all | solution.py:127
  203.0 6.8 %rev.20 = f32[1024,2,128]{2,0,1:T(8,128)S(1)} reverse(f32[1024,2,128]{2,0,1:T(8,128)} %copy_bitcast_fusion.1), dimensions={0} | reverse | bytes 2097152 | tf_op jit(solution)/shard_map/jit(_flip)/rev | solution.py:75
  218.3 6.2 %copy_bitcast_fusion = f32[1024,2,128]{2,0,1:T(8,128)} fusion(f32[256]{0:T(256)} %bitcast.284, f32[256]{0:T(256)} %bitcast.286, f32[256]{0:T(256)S(1)} %bitcast.276, f32[1024,256]{1,0:T(8,128)} %bitcast.240, f32[256]{0:T(256)S(1)} %bitcast.278, f32[256]{0:T(256)S(1)} %bitcast.280, f32[256]{0:T(256)} %bitcast.282, f32[256]{0:T(256)S(1)} %bitcast.274), kind=kLoop, calls=%fused_computation.43 | loop fusion | flops 4456448 | bytes 2104320 | tf_op jit(solution)/shard_map/reshape | solution.py:138
  224.5 6.8 %rev.21 = f32[1024,2,128]{2,0,1:T(8,128)S(1)} reverse(f32[1024,2,128]{2,0,1:T(8,128)} %copy_bitcast_fusion), dimensions={0} | reverse | bytes 2097152 | tf_op jit(solution)/shard_map/jit(_flip)/rev | solution.py:76
  241.9 18.6 %while.27 = (s32[]{:T(128)}, f32[2,2,64,128]{3,2,1,0:T(8,128)S(1)}, f32[8,2,2,64,128]{4,3,2,1,0:T(8,128)}, f32[8,2,2]{2,1,0:T(2,128)}, f32[8,2,2,64,128]{4,3,2,1,0:T(8,128)}, /*index=5*/s32[]{:T(128)}, s32[]{:T(128)}) while((s32[]{:T(128)}, f32[2,2,64,128]{3,2,1,0:T(8,128)S(1)}, f32[8,2,2,64,128]{4,3,2,1,0:T(8,128)}, ...), condition=%wide.region_5.6_spmd.clone, body=%wide.region_4.5_spmd.clone.sunk | while | flops 131075 | bytes 656016 | solution.py:61
  271.5 5.6 rev.22
  293.4 13.7 %while.26 = (s32[]{:T(128)}, f32[2,2,64,128]{3,2,1,0:T(8,128)S(1)}, f32[8,2,2,64,128]{4,3,2,1,0:T(8,128)S(1)}, f32[8,2,2]{2,1,0:T(2,128)}, f32[8,2,2,64,128]{4,3,2,1,0:T(8,128)}, /*index=5*/s32[]{:T(128)}, s32[]{:T(128)}) while((s32[]{:T(128)}, f32[2,2,64,128]{3,2,1,0:T(8,128)S(1)}, f32[8,2,2,64,128]{4,3,2,1,0:T(8,128)S(1)}, ...), condition=%wide.region_2.3_spmd.clone, body=%wide.region_1.2_spmd.clone.sunk | while | flops 131075 | bytes 655508 | solution.py:61
  309.4 5.6 fusion.24
  321.5 6.0 %all-to-all-start.4 = ((bf16[8,2,16384]{2,1,0:T(2,128)(2,1)}), bf16[8,2,16384]{2,1,0:T(2,128)(2,1)S(1)}, u32[]{:S(2)}, u32[]{:S(2)}) async-start(bf16[8,2,16384]{2,1,0:T(2,128)(2,1)} %reshape.337), calls=%async_computation.4 | async-start | bytes 1048576 | tf_op jit(solution)/shard_map/all_to_all | solution.py:146
  334.1 5.7 all-to-all-done.4
  348.9 6.0 %gather_fusion = bf16[1024,2048]{1,0:T(8,128)(2,1)} fusion(bf16[128,2048]{1,0:T(8,128)(2,1)S(1)} %multiply_convert_fusion.1, s32[1024]{0:T(1024)S(1)} %fusion.78), kind=kCustom, calls=%fused_computation | custom fusion | bytes 8392704 | tf_op jit(solution)/shard_map/gather | solution.py:180
  357.5 97.6 %all_to_all.28 = bf16[32,1,32,2048]{3,2,1,0:T(8,128)(2,1)S(1)} all-to-all(bf16[32,1,32,2048]{3,2,1,0:T(8,128)(2,1)S(1)} %broadcast_select_fusion), channel_id=1, replica_groups=mesh['sp'=8,'dp'=4] {'sp','dp'}, dimensions={0} | all-to-all | bytes 8388608 | tf_op jit(solution)/shard_map/all_to_all | solution.py:181
  459.7 5.7 multiply_convert_fusion
  465.3 6.1 %fusion.6 = bf16[1024,2048]{1,0:T(8,128)(2,1)} fusion(bf16[1024,1024]{1,0:T(8,128)(2,1)S(1)} %multiply_convert_fusion, bf16[1,1024,2048]{2,1,0:T(8,128)(2,1)S(1)} %copy-done.35), kind=kOutput, calls=%fused_computation.19 | convolution fusion | flops 4297064448 | bytes 10485760 | tf_op jit(solution)/shard_map/dot_general | solution.py:101
  475.6 94.1 %all-to-all-done.6 = bf16[1,32,32,2048]{3,2,0,1:T(8,128)(2,1)} async-done(((bf16[1,32,32,2048]{3,2,0,1:T(8,128)(2,1)}), bf16[1,32,32,2048]{3,2,0,1:T(8,128)(2,1)}, u32[]{:S(2)}, u32[]{:S(2)}) %all-to-all-start.6) | async-done | bytes 4194336 | tf_op jit(solution)/shard_map/all_to_all | solution.py:191
  569.7 7.1 %gather_fusion.1 = bf16[512,2048]{1,0:T(8,128)(2,1)S(1)} fusion(bf16[1024,2048]{1,0:T(8,128)(2,1)} %bitcast.69, s32[1024]{0:T(1024)S(1)} %pad_clamp_fusion), kind=kCustom, calls=%fused_computation.1 | custom fusion | bytes 4196352 | tf_op jit(solution)/shard_map/gather | solution.py:192
  (254 shorter events, 163.4 us)
Async XLA Ops:
  6.5 31.1 %copy-start.7 = (bf16[1,128,2048]{2,1,0:T(8,128)(2,1)S(1)}, bf16[1,128,2048]{2,1,0:T(8,128)(2,1)}, u32[]{:S(2)}) copy-start(bf16[1,128,2048]{2,1,0:T(8,128)(2,1)} %param.24) | copy-start | bytes 1572868
  9.2 55.2 %all-to-all-start.1 = ((bf16[8,2,512]{2,1,0:T(2,128)(2,1)}), bf16[8,2,512]{2,1,0:T(2,128)(2,1)S(1)}, u32[]{:S(2)}, u32[]{:S(2)}) async-start(bf16[8,2,512]{2,1,0:T(2,128)(2,1)} %reshape.329), calls=%async_computation.1 | async-start | bytes 32768 | tf_op jit(solution)/shard_map/all_to_all | solution.py:128
  16.5 327.5 %all-gather.2.cloned.1.call-start = ((), (), s32[]{:S(2)}) async-start(), calls=%async_computation.7 | async-start | bytes 10485760 | tf_op jit(solution)/shard_map/all_gather | solution.py:153
  22.7 28.1 %copy-start.8 = (bf16[1,128,2048]{2,1,0:T(8,128)(2,1)S(1)}, bf16[1,128,2048]{2,1,0:T(8,128)(2,1)}, u32[]{:S(2)}) copy-start(bf16[1,128,2048]{2,1,0:T(8,128)(2,1)} %param.25) | copy-start | bytes 1572868
  64.4 106.2 %all-to-all-start = ((bf16[8,2,16384]{2,1,0:T(2,128)(2,1)}), bf16[8,2,16384]{2,1,0:T(2,128)(2,1)}, u32[]{:S(2)}, u32[]{:S(2)}) async-start(bf16[8,2,16384]{2,1,0:T(2,128)(2,1)} %reshape.333), calls=%async_computation | async-start | bytes 1048576 | tf_op jit(solution)/shard_map/all_to_all | solution.py:125
  170.5 19.5 %all-to-all-start.2 = ((bf16[8,2,16384]{2,1,0:T(2,128)(2,1)}), bf16[8,2,16384]{2,1,0:T(2,128)(2,1)}, u32[]{:S(2)}, u32[]{:S(2)}) async-start(bf16[8,2,16384]{2,1,0:T(2,128)(2,1)} %reshape.331), calls=%async_computation.2 | async-start | bytes 1048576 | tf_op jit(solution)/shard_map/all_to_all | solution.py:126
  190.0 19.9 %all-to-all-start.3 = ((bf16[8,2,16384]{2,1,0:T(2,128)(2,1)}), bf16[8,2,16384]{2,1,0:T(2,128)(2,1)}, u32[]{:S(2)}, u32[]{:S(2)}) async-start(bf16[8,2,16384]{2,1,0:T(2,128)(2,1)} %reshape.335), calls=%async_computation.3 | async-start | bytes 1048576 | tf_op jit(solution)/shard_map/all_to_all | solution.py:127
  200.2 15.5 %copy-start = (f32[1,8,128,256]{3,2,1,0:T(8,128)}, f32[1,8,128,256]{3,2,1,0:T(8,128)S(1)}, u32[]{:S(2)}) copy-start(f32[1,8,128,256]{3,2,1,0:T(8,128)S(1)} %copy.175) | copy-start | bytes 3145732
  203.0 15.3 %copy-start.10 = (f32[1,256]{1,0:T(1,128)S(1)}, f32[1,256]{1,0:T(1,128)}, u32[]{:S(2)}) copy-start(f32[1,256]{1,0:T(1,128)} %get-tuple-element.177) | copy-start | bytes 3076
  203.0 15.3 %copy-start.11 = (f32[1,256]{1,0:T(1,128)S(1)}, f32[1,256]{1,0:T(1,128)}, u32[]{:S(2)}) copy-start(f32[1,256]{1,0:T(1,128)} %get-tuple-element.178) | copy-start | bytes 3076
  203.0 15.3 %copy-start.12 = (f32[1,256]{1,0:T(1,128)S(1)}, f32[1,256]{1,0:T(1,128)}, u32[]{:S(2)}) copy-start(f32[1,256]{1,0:T(1,128)} %get-tuple-element.179) | copy-start | bytes 3076
  203.0 15.3 %copy-start.13 = (f32[1,256]{1,0:T(1,128)S(1)}, f32[1,256]{1,0:T(1,128)}, u32[]{:S(2)}) copy-start(f32[1,256]{1,0:T(1,128)} %get-tuple-element.180) | copy-start | bytes 3076
  240.8 23.3 %copy-start.3 = (f32[32,8,8,128]{3,2,1,0:T(8,128)S(1)}, f32[32,8,8,128]{3,2,1,0:T(8,128)}, u32[]{:S(2)}) copy-start(f32[32,8,8,128]{3,2,1,0:T(8,128)} %copy.245) | copy-start | bytes 3145732
  269.6 8.7 %copy-start.1 = (f32[1,8,128,256]{3,2,1,0:T(8,128)S(1)}, f32[1,8,128,256]{3,2,1,0:T(8,128)}, u32[]{:S(2)}) copy-start(f32[1,8,128,256]{3,2,1,0:T(8,128)} %copy-done) | copy-start | bytes 3145732
  269.6 8.7 %copy-start.19 = (f32[1,256]{1,0:T(1,128)S(1)}, f32[1,256]{1,0:T(1,128)}, u32[]{:S(2)}) copy-start(f32[1,256]{1,0:T(1,128)} %get-tuple-element.191) | copy-start | bytes 3076
  269.6 8.7 %copy-start.21 = (f32[1,256]{1,0:T(1,128)S(1)}, f32[1,256]{1,0:T(1,128)}, u32[]{:S(2)}) copy-start(f32[1,256]{1,0:T(1,128)} %get-tuple-element.192) | copy-start | bytes 3076
  269.6 8.7 %copy-start.23 = (f32[1,256]{1,0:T(1,128)S(1)}, f32[1,256]{1,0:T(1,128)}, u32[]{:S(2)}) copy-start(f32[1,256]{1,0:T(1,128)} %get-tuple-element.193) | copy-start | bytes 3076
  293.3 16.1 %copy-start.6 = (f32[8,128,2,2,64]{1,0,4,3,2:T(8,128)S(1)}, f32[8,128,2,2,64]{1,0,4,3,2:T(8,128)}, u32[]{:S(2)}) copy-start(f32[8,128,2,2,64]{1,0,4,3,2:T(8,128)} %get-tuple-element.170) | copy-start | bytes 3145732
  315.9 11.6 %copy-start.9 = (bf16[1,128,2048]{2,1,0:T(8,128)(2,1)S(1)}, bf16[1,128,2048]{2,1,0:T(8,128)(2,1)}, u32[]{:S(2)}) copy-start(bf16[1,128,2048]{2,1,0:T(8,128)(2,1)} %param.27) | copy-start | bytes 1572868
  315.9 12.1 %copy-start.31 = (s32[1,128,4]{1,2,0:T(4,128)S(1)}, s32[1,128,4]{1,2,0:T(4,128)}, u32[]{:S(2)}) copy-start(s32[1,128,4]{1,2,0:T(4,128)} %param.35) | copy-start | bytes 6148
  321.5 18.2 %all-to-all-start.4 = ((bf16[8,2,16384]{2,1,0:T(2,128)(2,1)}), bf16[8,2,16384]{2,1,0:T(2,128)(2,1)S(1)}, u32[]{:S(2)}, u32[]{:S(2)}) async-start(bf16[8,2,16384]{2,1,0:T(2,128)(2,1)} %reshape.337), calls=%async_computation.4 | async-start | bytes 1048576 | tf_op jit(solution)/shard_map/all_to_all | solution.py:146
  328.3 15.3 %copy-start.29 = (f32[2048]{0:T(1024)S(1)}, f32[2048]{0:T(1024)}, u32[]{:S(2)}) copy-start(f32[2048]{0:T(1024)} %param.32) | copy-start | bytes 24580
  357.5 97.6 %copy-start.33 = (bf16[1,2048,1024]{2,1,0:T(8,128)(2,1)S(1)}, bf16[1,2048,1024]{2,1,0:T(8,128)(2,1)}, u32[]{:S(2)}) copy-start(bf16[1,2048,1024]{2,1,0:T(8,128)(2,1)} %param.37) | copy-start | bytes 12582916
  471.5 98.2 %all-to-all-start.6 = ((bf16[1,32,32,2048]{3,2,0,1:T(8,128)(2,1)}), bf16[1,32,32,2048]{3,2,0,1:T(8,128)(2,1)}, u32[]{:S(2)}, u32[]{:S(2)}) async-start(bf16[1,32,32,2048]{3,2,0,1:T(8,128)(2,1)} %bitcast.249), calls=%async_computation.6 | async-start | bytes 8388608 | tf_op jit(solution)/shard_map/all_to_all | solution.py:191
  (19 other events, 126.1 us)
Sparse Core Ops, SparseCore 0:
  18.9 59.6 all-gather.1
where the time goes:
time: 604 us; the launch traced here: 593 us
  other arithmetic  188 us (31%)
  local copies, waits for them, and re-layouts  107 us (18%)
  waiting for transfers between devices  101 us (17%)
  blocking collectives  97.6 us (16%)
  matrix products  49.4 us (8%)
  starting transfers between devices  35.4 us (6%)
  between operations  14.5 us (2%)
    all_to_all x1, blocking collectives, per_device(): lax.all_to_all(outgoing.reshape(experts_all, 1, capacity, model_width), (...  97.6 us
    another operation x2, other arithmetic, ssd_direction(): jnp.cumsum((-step_size * rates).reshape(blocks, BLOCK, group_count, per_g...  94.9 us
    all_to_all x1, waiting for transfers between devices, per_device(): lax.all_to_all(served, ('sp', 'dp'), split_axis=1, concat_axis=0, tiled=T...  94.1 us
    unnamed x8, other arithmetic  39.5 us
    unnamed x95, local copies, waits for them, and re-layouts  22.3 us
    add x16, other arithmetic, advance(): return (factor[..., None, None] * running + block_state, running)  15.7 us
  transfers between devices with their start and end apart: 7, of which 3 were waited for; matrix products, arithmetic and copies ran while one was open for 50% of the time, Pallas kernels for 0%

commit v1 on v0

--- a/solution.py
+++ b/solution.py
@@ -188,7 +188,9 @@
     served = expert_apply(arrived.reshape(-1, model_width), gate_w[0], up_w[0], down_w[0]).reshape(
         arrived.shape
     )
-    returned = lax.all_to_all(served, ("sp", "dp"), split_axis=1, concat_axis=0, tiled=True)
+    parts = jnp.split(served, lax.axis_size(("sp", "dp")), axis=1)
+    got = lax.all_to_all(jnp.stack(parts), ("sp", "dp"), 0, 0)
+    returned = jnp.concatenate(got, axis=0)
     answers = returned.reshape(experts_all * capacity, model_width)[target].reshape(
         token_count, top_count, model_width
     )

time: 604 us -> 624 us (1.033)
  local copies, waits for them, and re-layouts: 107 us -> 128 us
    unnamed x95 -> x126, local copies, waits for them, and re-layouts: 22.3 us -> 42.9 us
  transfers between devices with their start and end apart: 7 -> 7, of which waited for: 3 -> 3; matrix products, arithmetic and copies ran while one was open for 50% -> 48% of each run, Pallas kernels for 0% -> 0%
where the time goes in v1:
time: 624 us; the launch traced here: 613 us
  other arithmetic  187 us (30%)
  local copies, waits for them, and re-layouts  128 us (21%)
  waiting for transfers between devices  101 us (16%)
  blocking collectives  97.4 us (16%)
  matrix products  48 us (8%)
  starting transfers between devices  35.3 us (6%)
  between operations  14.9 us (2%)
    all_to_all x1, blocking collectives, per_device(): lax.all_to_all(outgoing.reshape(experts_all, 1, capacity, model_width), (...  97.4 us
    another operation x2, other arithmetic, ssd_direction(): jnp.cumsum((-step_size * rates).reshape(blocks, BLOCK, group_count, per_g...  94.9 us
    all_to_all x1, waiting for transfers between devices, per_device(): got = lax.all_to_all(jnp.stack(parts), ('sp', 'dp'), 0, 0)  94.1 us
    unnamed x126, local copies, waits for them, and re-layouts  42.9 us
    unnamed x8, other arithmetic  39.3 us
    add x16, other arithmetic, advance(): return (factor[..., None, None] * running + block_state, running)  15.7 us
  transfers between devices with their start and end apart: 7, of which 3 were waited for; matrix products, arithmetic and copies ran while one was open for 48% of the time, Pallas kernels for 0%

profile of v1, /device:TPU:0, one launch (start us, length us, event | category | flops | bytes accessed | tf_op | source)
XLA Modules:
  0.0 613.1 jit_solution(1986890154848243864)
XLA Ops:
  9.2 7.3 %all-to-all-start.1 = ((bf16[8,2,512]{2,1,0:T(2,128)(2,1)}), bf16[8,2,512]{2,1,0:T(2,128)(2,1)S(1)}, u32[]{:S(2)}, u32[]{:S(2)}) async-start(bf16[8,2,512]{2,1,0:T(2,128)(2,1)} %reshape.321), calls=%async_computation.1 | async-start | bytes 32768 | tf_op jit(solution)/shard_map/all_to_all | solution.py:128
  25.2 11.5 %reduce.8 = bf16[2048,128]{1,0:T(8,128)(2,1)S(1)} reduce(bf16[2048,1,128]{2,1,0:T(2,128)(2,1)S(1)} %bitcast.413, bf16[]{:T(256)} %broadcast.189), dimensions={1}, to_apply=%bitcast.319.reduce_sub_computation | reduce | bytes 1048578
  38.4 11.5 %reduce.7 = bf16[2048,128]{1,0:T(8,128)(2,1)S(1)} reduce(bf16[2048,1,128]{2,1,0:T(2,128)(2,1)S(1)} %bitcast.414, bf16[]{:T(256)} %broadcast.189), dimensions={1}, to_apply=%bitcast.317.reduce_sub_computation | reduce | bytes 1048578
  51.6 11.7 %reduce.9 = bf16[2048,128]{1,0:T(8,128)(2,1)S(1)} reduce(bf16[2048,1,128]{2,1,0:T(2,128)(2,1)S(1)} %bitcast.415, bf16[]{:T(256)} %broadcast.189), dimensions={1}, to_apply=%bitcast.321.reduce_sub_computation | reduce | bytes 1048578
  64.3 6.0 all-to-all-start
  71.7 47.4 %fusion.127 = f32[8,128,2,2]{3,0,1,2:T(8,128)S(1)} fusion(f32[8,128,2,2]{3,0,1,2:T(8,128)S(1)} %copy.202), kind=kOutput, calls=%fused_computation.219 | output fusion | flops 520192 | bytes 32768 | tf_op jit(solution)/shard_map/jit(cumsum)/reduce_window_sum | solution.py:36
  119.8 47.4 %fusion.126 = f32[8,128,2,2]{3,0,1,2:T(8,128)S(1)} fusion(f32[8,128,2,2]{3,0,1,2:T(8,128)S(1)} %copy.183), kind=kOutput, calls=%fused_computation.218 | output fusion | flops 520192 | bytes 32768 | tf_op jit(solution)/shard_map/jit(cumsum)/reduce_window_sum | solution.py:36
  170.4 6.0 all-to-all-start.2
  189.9 5.9 all-to-all-start.3
  202.6 6.8 %rev.20 = f32[1024,2,128]{2,0,1:T(8,128)S(1)} reverse(f32[1024,2,128]{2,0,1:T(8,128)} %copy_bitcast_fusion.1), dimensions={0} | reverse | bytes 2097152 | tf_op jit(solution)/shard_map/jit(_flip)/rev | solution.py:75
  217.9 6.2 %copy_bitcast_fusion = f32[1024,2,128]{2,0,1:T(8,128)} fusion(f32[256]{0:T(256)} %bitcast.441, f32[256]{0:T(256)} %bitcast.443, f32[256]{0:T(256)S(1)} %bitcast.433, f32[1024,256]{1,0:T(8,128)} %bitcast.366, f32[256]{0:T(256)S(1)} %bitcast.435, f32[256]{0:T(256)S(1)} %bitcast.437, f32[256]{0:T(256)} %bitcast.439, f32[256]{0:T(256)S(1)} %bitcast.431), kind=kLoop, calls=%fused_computation.43 | loop fusion | flops 4456448 | bytes 2104320 | tf_op jit(solution)/shard_map/reshape | solution.py:138
  224.1 6.8 %rev.21 = f32[1024,2,128]{2,0,1:T(8,128)S(1)} reverse(f32[1024,2,128]{2,0,1:T(8,128)} %copy_bitcast_fusion), dimensions={0} | reverse | bytes 2097152 | tf_op jit(solution)/shard_map/jit(_flip)/rev | solution.py:76
  241.5 18.9 %while.27 = (s32[]{:T(128)}, f32[2,2,64,128]{3,2,1,0:T(8,128)S(1)}, f32[8,2,2,64,128]{4,3,2,1,0:T(8,128)}, f32[8,2,2]{2,1,0:T(2,128)}, f32[8,2,2,64,128]{4,3,2,1,0:T(8,128)}, /*index=5*/s32[]{:T(128)}, s32[]{:T(128)}) while((s32[]{:T(128)}, f32[2,2,64,128]{3,2,1,0:T(8,128)S(1)}, f32[8,2,2,64,128]{4,3,2,1,0:T(8,128)}, ...), condition=%wide.region_5.6_spmd.clone, body=%wide.region_4.5_spmd.clone.sunk | while | flops 131075 | bytes 656016 | solution.py:61
  263.9 5.5 fusion.30
  271.3 5.6 rev.22
  293.2 13.6 %while.26 = (s32[]{:T(128)}, f32[2,2,64,128]{3,2,1,0:T(8,128)S(1)}, f32[8,2,2,64,128]{4,3,2,1,0:T(8,128)S(1)}, f32[8,2,2]{2,1,0:T(2,128)}, f32[8,2,2,64,128]{4,3,2,1,0:T(8,128)}, /*index=5*/s32[]{:T(128)}, s32[]{:T(128)}) while((s32[]{:T(128)}, f32[2,2,64,128]{3,2,1,0:T(8,128)S(1)}, f32[8,2,2,64,128]{4,3,2,1,0:T(8,128)S(1)}, ...), condition=%wide.region_2.3_spmd.clone, body=%wide.region_1.2_spmd.clone.sunk | while | flops 131075 | bytes 655508 | solution.py:61
  309.1 5.6 fusion.24
  321.3 6.0 all-to-all-start.4
  333.8 5.7 all-to-all-done.4
  348.7 6.0 gather_fusion
  357.3 97.4 %all_to_all.28 = bf16[32,1,32,2048]{3,2,1,0:T(8,128)(2,1)S(1)} all-to-all(bf16[32,1,32,2048]{3,2,1,0:T(8,128)(2,1)S(1)} %broadcast_select_fusion), channel_id=1, replica_groups=mesh['sp'=8,'dp'=4] {'sp','dp'}, dimensions={0} | all-to-all | bytes 8388608 | tf_op jit(solution)/shard_map/all_to_all | solution.py:181
  459.2 5.7 multiply_convert_fusion
  495.2 94.1 %all-to-all-done.6 = bf16[32,1,1,32,2048]{4,3,2,1,0:T(8,128)(2,1)} async-done(((bf16[32,1,1,32,2048]{4,3,2,1,0:T(8,128)(2,1)}), bf16[32,1,1,32,2048]{4,3,2,1,0:T(8,128)(2,1)}, u32[]{:S(2)}, u32[]{:S(2)}) %all-to-all-start.6) | async-done | bytes 4194336 | tf_op jit(solution)/shard_map/all_to_all | solution.py:192
  589.3 7.1 %gather_fusion.1 = bf16[512,2048]{1,0:T(8,128)(2,1)S(1)} fusion(bf16[1024,2048]{1,0:T(8,128)(2,1)} %bitcast.100, s32[1024]{0:T(1024)S(1)} %pad_clamp_fusion), kind=kCustom, calls=%fused_computation.1 | custom fusion | bytes 4196352 | tf_op jit(solution)/shard_map/gather | solution.py:194
  (286 shorter events, 184.0 us)
Async XLA Ops:
  6.5 31.1 %copy-start.7 = (bf16[1,128,2048]{2,1,0:T(8,128)(2,1)S(1)}, bf16[1,128,2048]{2,1,0:T(8,128)(2,1)}, u32[]{:S(2)}) copy-start(bf16[1,128,2048]{2,1,0:T(8,128)(2,1)} %param.24) | copy-start | bytes 1572868
  9.2 55.0 %all-to-all-start.1 = ((bf16[8,2,512]{2,1,0:T(2,128)(2,1)}), bf16[8,2,512]{2,1,0:T(2,128)(2,1)S(1)}, u32[]{:S(2)}, u32[]{:S(2)}) async-start(bf16[8,2,512]{2,1,0:T(2,128)(2,1)} %reshape.321), calls=%async_computation.1 | async-start | bytes 32768 | tf_op jit(solution)/shard_map/all_to_all | solution.py:128
  16.5 327.2 %all-gather.2.cloned.1.call-start = ((), (), s32[]{:S(2)}) async-start(), calls=%async_computation.7 | async-start | bytes 10485760 | tf_op jit(solution)/shard_map/all_gather | solution.py:153
  22.7 28.1 %copy-start.8 = (bf16[1,128,2048]{2,1,0:T(8,128)(2,1)S(1)}, bf16[1,128,2048]{2,1,0:T(8,128)(2,1)}, u32[]{:S(2)}) copy-start(bf16[1,128,2048]{2,1,0:T(8,128)(2,1)} %param.25) | copy-start | bytes 1572868
  64.3 106.2 %all-to-all-start = ((bf16[8,2,16384]{2,1,0:T(2,128)(2,1)}), bf16[8,2,16384]{2,1,0:T(2,128)(2,1)}, u32[]{:S(2)}, u32[]{:S(2)}) async-start(bf16[8,2,16384]{2,1,0:T(2,128)(2,1)} %reshape.325), calls=%async_computation | async-start | bytes 1048576 | tf_op jit(solution)/shard_map/all_to_all | solution.py:125
  170.4 19.5 %all-to-all-start.2 = ((bf16[8,2,16384]{2,1,0:T(2,128)(2,1)}), bf16[8,2,16384]{2,1,0:T(2,128)(2,1)}, u32[]{:S(2)}, u32[]{:S(2)}) async-start(bf16[8,2,16384]{2,1,0:T(2,128)(2,1)} %reshape.323), calls=%async_computation.2 | async-start | bytes 1048576 | tf_op jit(solution)/shard_map/all_to_all | solution.py:126
  189.9 19.6 %all-to-all-start.3 = ((bf16[8,2,16384]{2,1,0:T(2,128)(2,1)}), bf16[8,2,16384]{2,1,0:T(2,128)(2,1)}, u32[]{:S(2)}, u32[]{:S(2)}) async-start(bf16[8,2,16384]{2,1,0:T(2,128)(2,1)} %reshape.327), calls=%async_computation.3 | async-start | bytes 1048576 | tf_op jit(solution)/shard_map/all_to_all | solution.py:127
  199.8 15.5 %copy-start = (f32[1,8,128,256]{3,2,1,0:T(8,128)}, f32[1,8,128,256]{3,2,1,0:T(8,128)S(1)}, u32[]{:S(2)}) copy-start(f32[1,8,128,256]{3,2,1,0:T(8,128)S(1)} %copy.175) | copy-start | bytes 3145732
  202.6 15.3 %copy-start.10 = (f32[1,256]{1,0:T(1,128)S(1)}, f32[1,256]{1,0:T(1,128)}, u32[]{:S(2)}) copy-start(f32[1,256]{1,0:T(1,128)} %get-tuple-element.177) | copy-start | bytes 3076
  202.6 15.3 %copy-start.11 = (f32[1,256]{1,0:T(1,128)S(1)}, f32[1,256]{1,0:T(1,128)}, u32[]{:S(2)}) copy-start(f32[1,256]{1,0:T(1,128)} %get-tuple-element.178) | copy-start | bytes 3076
  202.6 15.3 %copy-start.12 = (f32[1,256]{1,0:T(1,128)S(1)}, f32[1,256]{1,0:T(1,128)}, u32[]{:S(2)}) copy-start(f32[1,256]{1,0:T(1,128)} %get-tuple-element.179) | copy-start | bytes 3076
  202.6 15.3 %copy-start.13 = (f32[1,256]{1,0:T(1,128)S(1)}, f32[1,256]{1,0:T(1,128)}, u32[]{:S(2)}) copy-start(f32[1,256]{1,0:T(1,128)} %get-tuple-element.180) | copy-start | bytes 3076
  240.4 23.5 %copy-start.3 = (f32[32,8,8,128]{3,2,1,0:T(8,128)S(1)}, f32[32,8,8,128]{3,2,1,0:T(8,128)}, u32[]{:S(2)}) copy-start(f32[32,8,8,128]{3,2,1,0:T(8,128)} %copy.244) | copy-start | bytes 3145732
  269.4 8.7 %copy-start.1 = (f32[1,8,128,256]{3,2,1,0:T(8,128)S(1)}, f32[1,8,128,256]{3,2,1,0:T(8,128)}, u32[]{:S(2)}) copy-start(f32[1,8,128,256]{3,2,1,0:T(8,128)} %copy-done) | copy-start | bytes 3145732
  269.4 8.7 %copy-start.19 = (f32[1,256]{1,0:T(1,128)S(1)}, f32[1,256]{1,0:T(1,128)}, u32[]{:S(2)}) copy-start(f32[1,256]{1,0:T(1,128)} %get-tuple-element.191) | copy-start | bytes 3076
  269.4 8.7 %copy-start.21 = (f32[1,256]{1,0:T(1,128)S(1)}, f32[1,256]{1,0:T(1,128)}, u32[]{:S(2)}) copy-start(f32[1,256]{1,0:T(1,128)} %get-tuple-element.192) | copy-start | bytes 3076
  269.4 8.7 %copy-start.23 = (f32[1,256]{1,0:T(1,128)S(1)}, f32[1,256]{1,0:T(1,128)}, u32[]{:S(2)}) copy-start(f32[1,256]{1,0:T(1,128)} %get-tuple-element.193) | copy-start | bytes 3076
  293.0 16.1 %copy-start.6 = (f32[8,128,2,2,64]{1,0,4,3,2:T(8,128)S(1)}, f32[8,128,2,2,64]{1,0,4,3,2:T(8,128)}, u32[]{:S(2)}) copy-start(f32[8,128,2,2,64]{1,0,4,3,2:T(8,128)} %get-tuple-element.170) | copy-start | bytes 3145732
  315.7 11.6 %copy-start.9 = (bf16[1,128,2048]{2,1,0:T(8,128)(2,1)S(1)}, bf16[1,128,2048]{2,1,0:T(8,128)(2,1)}, u32[]{:S(2)}) copy-start(bf16[1,128,2048]{2,1,0:T(8,128)(2,1)} %param.27) | copy-start | bytes 1572868
  315.7 12.1 %copy-start.31 = (s32[1,128,4]{1,2,0:T(4,128)S(1)}, s32[1,128,4]{1,2,0:T(4,128)}, u32[]{:S(2)}) copy-start(s32[1,128,4]{1,2,0:T(4,128)} %param.35) | copy-start | bytes 6148
  321.3 18.2 %all-to-all-start.4 = ((bf16[8,2,16384]{2,1,0:T(2,128)(2,1)}), bf16[8,2,16384]{2,1,0:T(2,128)(2,1)S(1)}, u32[]{:S(2)}, u32[]{:S(2)}) async-start(bf16[8,2,16384]{2,1,0:T(2,128)(2,1)} %reshape.329), calls=%async_computation.4 | async-start | bytes 1048576 | tf_op jit(solution)/shard_map/all_to_all | solution.py:146
  328.0 15.3 %copy-start.29 = (f32[2048]{0:T(1024)S(1)}, f32[2048]{0:T(1024)}, u32[]{:S(2)}) copy-start(f32[2048]{0:T(1024)} %param.32) | copy-start | bytes 24580
  357.2 97.4 %copy-start.33 = (bf16[1,2048,1024]{2,1,0:T(8,128)(2,1)S(1)}, bf16[1,2048,1024]{2,1,0:T(8,128)(2,1)}, u32[]{:S(2)}) copy-start(bf16[1,2048,1024]{2,1,0:T(8,128)(2,1)} %param.37) | copy-start | bytes 12582916
  491.0 98.3 %all-to-all-start.6 = ((bf16[32,1,1,32,2048]{4,3,2,1,0:T(8,128)(2,1)}), bf16[32,1,1,32,2048]{4,3,2,1,0:T(8,128)(2,1)}, u32[]{:S(2)}, u32[]{:S(2)}) async-start(bf16[32,1,1,32,2048]{4,3,2,1,0:T(8,128)(2,1)} %fusion.76), calls=%async_computation.6 | async-start | bytes 8388608 | tf_op jit(solution)/shard_map/all_to_all | solution.py:192
  (19 other events, 126.2 us)
Sparse Core Ops, SparseCore 0:
  18.9 59.6 all-gather.1
